TPU v7x, 32 devices: a whole 2x2x4 slice. The times are simulated.
32 devices in a mesh: sp: 16 (over z, y, x), tp: 2 (over core).
Axes of the slice: x: 2, y: 2, z: 4, core: 2. Of those that a mesh axis runs over, the one named last changes fastest.
Arguments:
- residual: bfloat16 [3072, 2048], P(('sp', 'tp')), may hold values from -6 to 6
- queries: bfloat16 [3072, 1024], P('sp', 'tp'), may hold values from -6 to 6
- key_pairs: bfloat16 [3072, 1024], P('sp', 'tp'), may hold values from -6 to 6
- values: bfloat16 [3072, 1024], P('sp', 'tp'), may hold values from -6 to 6
- second_weight: float32 [8], P('tp'), may hold values from 0.3 to 0.8
- head_gain: float32 [1024], P('tp'), may hold values from 0.1 to 1.9
- out_weight: bfloat16 [1024, 2048], P('tp'), may hold values from -0.1875 to 0.1875
- norm_gain: float32 [2048], replicated, may hold values from 0.1 to 1.9
- up_weight: bfloat16 [2048, 5632], P('sp', 'tp'), may hold values from -0.125 to 0.125
- gate_weight: bfloat16 [2048, 5632], P('sp', 'tp'), may hold values from -0.125 to 0.125
- conv_weight: float32 [3, 5632], P(None, 'tp'), may hold values from -3.5 to 3.5
- conv_bias: float32 [5632], P('tp'), may hold values from -3 to 3
- down_weight: bfloat16 [5632, 2048], P('tp', 'sp'), may hold values from -0.078125 to 0.078125
Outputs:
- layer_out: bfloat16 [3072, 2048], P(('sp', 'tp'))
All inputs are finite; a program needn't handle non-finite values.
Results may differ from a plain program's by a relative error of at most 0.017.
Values may be sent and summed in bfloat16 or wider, within the bound.
A program may use at most 128 MiB of HBM per device.

v0:
```python
import jax
import jax.numpy as jnp
from jax import lax
from jax.sharding import PartitionSpec as P

HD = 64
VD = 128


eps = 1e-05
neg_fill = -1e30


def from_behind(value, axis, steps):
    count = lax.axis_size(axis)
    leading, last = (max(0, -steps), min(count, count - steps))
    return lax.ppermute(value, axis, [(source, source + steps) for source in range(leading, last)])


def normalize(rows_in, gain):
    values_f = rows_in.astype(jnp.float32)
    scale_inv = lax.rsqrt(jnp.mean(values_f * values_f, axis=-1, keepdims=True) + eps)
    return (values_f * scale_inv * gain).astype(jnp.bfloat16)


def local(
    residual,
    queries,
    key_pairs,
    values,
    second_weight,
    head_gain,
    out_weight,
    norm_gain,
    up_weight,
    gate_weight,
    conv_weight,
    conv_bias,
    down_weight,
):
    tok_rows = queries.shape[0]
    head_count = second_weight.shape[0]
    ff_local = up_weight.shape[1]
    sp_index = lax.axis_index("sp")
    query = queries.reshape(tok_rows, head_count, 2, HD)
    query_pos = sp_index * tok_rows + jnp.arange(tok_rows)
    last_query = (sp_index + 1) * tok_rows
    initial = (
        jnp.full((head_count, 2, tok_rows), neg_fill, jnp.float32),
        jnp.zeros((head_count, 2, tok_rows), jnp.float32),
        jnp.zeros((head_count, 2, tok_rows, VD), jnp.float32),
    )
    key_piece = lax.all_gather(key_pairs, "sp", axis=0, tiled=True)
    value_piece = lax.all_gather(values, "sp", axis=0, tiled=True)
    piece_len = key_piece.shape[0]

    def compute(state_in):
        maxima, totals, weighted = state_in
        key_rows = key_piece.reshape(piece_len, head_count, 2, HD)
        value_rows = value_piece.reshape(piece_len, head_count, VD)
        scores = jnp.einsum(
            "qhmd,khmd->hmqk", query, key_rows, preferred_element_type=jnp.float32
        ) * HD ** (-0.5)
        visible = jnp.arange(piece_len)[None, :] <= query_pos[:, None]
        scores = jnp.where(visible, scores, neg_fill)
        new_max = jnp.maximum(maxima, jnp.max(scores, axis=-1))
        exp_scores = jnp.where(visible, jnp.exp(scores - new_max[..., None]), jnp.float32(0.0))
        totals = jnp.sum(exp_scores, axis=-1)
        weighted = jnp.einsum(
            "hmqk,khe->hmqe",
            exp_scores.astype(jnp.bfloat16),
            value_rows,
            preferred_element_type=jnp.float32,
        )
        return (new_max, totals, weighted)

    def keep_state(state_in):
        return state_in

    maxima, totals, weighted = lax.cond(jnp.int32(0) < last_query, compute, keep_state, initial)
    diff = (
        weighted[:, 0] / totals[:, 0, :, None]
        - second_weight[:, None, None] * weighted[:, 1] / totals[:, 1, :, None]
    )
    diff = jnp.transpose(diff, (1, 0, 2))
    scale_inv = lax.rsqrt(jnp.mean(diff * diff, axis=-1, keepdims=True) + eps)
    attended = (
        (diff * scale_inv * head_gain.reshape(head_count, VD) * 0.8)
        .reshape(tok_rows, head_count * VD)
        .astype(jnp.bfloat16)
    )
    proj = lax.psum_scatter(
        jnp.dot(attended, out_weight, preferred_element_type=jnp.float32).astype(jnp.bfloat16),
        "tp",
        scatter_dimension=0,
        tiled=True,
    )
    mid = (residual.astype(jnp.float32) + proj.astype(jnp.float32)).astype(jnp.bfloat16)
    normed_all = lax.all_gather(normalize(mid, norm_gain), "tp", axis=0, tiled=True)
    up_sum = jnp.dot(
        normed_all,
        lax.all_gather(up_weight, "sp", axis=0, tiled=True),
        preferred_element_type=jnp.float32,
    )
    gate_sum = jnp.dot(
        normed_all,
        lax.all_gather(gate_weight, "sp", axis=0, tiled=True),
        preferred_element_type=jnp.float32,
    )
    up_proj = up_sum.astype(jnp.bfloat16)
    gate_proj = gate_sum.astype(jnp.bfloat16)
    taps = conv_weight.shape[0]
    rim_rows = from_behind(up_proj[tok_rows - (taps - 1) :], "sp", 1)
    extended = jnp.concatenate((rim_rows, up_proj), axis=0)
    conv_out = jnp.zeros((tok_rows, ff_local), jnp.float32) + conv_bias[None, :]
    for tap in range(taps):
        conv_out = conv_out + conv_weight[tap][None, :] * extended[tap : tap + tok_rows].astype(
            jnp.float32
        )
    hidden = (jax.nn.silu(conv_out) * gate_proj.astype(jnp.float32)).astype(jnp.bfloat16)
    down_all = lax.all_gather(down_weight, "sp", axis=1, tiled=True)
    ffn_out = lax.psum_scatter(
        jnp.dot(hidden, down_all, preferred_element_type=jnp.float32).astype(jnp.bfloat16),
        "tp",
        scatter_dimension=0,
        tiled=True,
    )
    return (mid.astype(jnp.float32) + ffn_out.astype(jnp.float32)).astype(jnp.bfloat16)


def solution(mesh):
    return jax.shard_map(
        local,
        mesh=mesh,
        in_specs=(
            P(("sp", "tp"), None),
            P("sp", "tp"),
            P("sp", "tp"),
            P("sp", "tp"),
            P("tp"),
            P("tp"),
            P("tp", None),
            P(),
            P("sp", "tp"),
            P("sp", "tp"),
            P(None, "tp"),
            P("tp"),
            P("tp", "sp"),
        ),
        out_specs=P(("sp", "tp"), None),
        check_vma=False,
    )
```

profile of v0, /device:TPU:15, one launch (start us, length us, event | category | flops | bytes accessed | tf_op | source)
XLA Modules:
  0.0 704.0 jit_solution(9887044699763358971)
XLA Ops:
  6.5 0.7 all-gather.6.cloned.1.call-update
  7.3 0.7 all-gather.8.cloned.1.call-update
  8.1 69.1 %all-gather.6.cloned.1.call-done = bf16[3072,512]{1,0:T(8,128)(2,1)} async-done(((bf16[192,512]{1,0:T(8,128)(2,1)}), bf16[3072,512]{1,0:T(8,128)(2,1)}) %all-gather.6.cloned.1.call-update) | async-done | bytes 3145744 | tf_op jit(solution)/shard_map/all_gather | solution.py:53
  77.2 69.2 %all-gather.8.cloned.1.call-done = bf16[3072,512]{1,0:T(8,128)(2,1)} async-done(((bf16[192,512]{1,0:T(8,128)(2,1)}), bf16[3072,512]{1,0:T(8,128)(2,1)}) %all-gather.8.cloned.1.call-update) | async-done | bytes 3145744 | tf_op jit(solution)/shard_map/all_gather | solution.py:54
  146.4 45.3 %conditional.1 = (f32[4,2,192]{2,1,0:T(2,128)S(1)}, f32[4,2,192,128]{3,2,1,0:T(8,128)S(1)}) conditional(s32[]{:T(128)} %convert_element_type.62, () %tuple.13, (s32[]{:T(128)}, s32[192]{0:T(256)S(1)}, bf16[192,512]{1,0:T(8,128)(2,1)}, bf16[3072,512]{1,0:T(8,128)(2,1)}, bf16[3072,512]{1,0:T(8,128)(2,1)}) %tuple.14), branch_computations={%region_0.0_spmd, %region_1.4_spmd} | conditional | flops 1873869568 | bytes 80058688 | solution.py:80
  146.8 4.8 copy.26
  151.7 11.8 %fusion = (f32[4,2,192]{2,1,0:T(2,128)S(1)}, f32[4,2,192,3072]{3,2,1,0:T(8,128)}) fusion(pred[192,3072]{1,0:T(8,128)(4,1)S(1)} %iota_compare_fusion, bf16[192,4,2,64]{0,3,2,1:T(8,128)(2,1)S(1)} %bitcast.44, bf16[3072,4,2,64]{0,3,2,1:T(8,128)(2,1)} %bitcast.42), kind=kOutput, calls=%fused_computation.2 | convolution fusion | flops 618134016 | bytes 22812672 | tf_op jit(solution)/shard_map/cond/branch_1_fun/qhmd,khmd->hmqk/dot_general | solution.py:61
  163.5 5.5 reshape.37
  169.0 10.7 %fusion.3 = f32[4,2,192,128]{3,2,1,0:T(8,128)S(1)} fusion(f32[4,2,192,3072]{3,2,1,0:T(8,128)} %get-tuple-element.52, f32[4,2,192]{2,1,0:T(2,128)S(1)} %broadcast_maximum_fusion, pred[192,3072]{1,0:T(8,128)(4,1)S(1)} %iota_compare_fusion, bf16[3072,4,128,1]{2,1,0,3:T(4,128)(2,1)} %bitcast.43), kind=kOutput, calls=%fused_computation.5 | convolution fusion | flops 1231552512 | bytes 23402496 | tf_op jit(solution)/shard_map/cond/branch_1_fun/hmqk,khe->hmqe/dot_general | solution.py:69
  179.7 11.9 %fusion.2 = f32[4,2,192]{2,1,0:T(2,128)S(1)} fusion(f32[4,2,192,3072]{3,2,1,0:T(8,128)} %get-tuple-element.52, f32[4,2,192]{2,1,0:T(2,128)S(1)} %broadcast_maximum_fusion, pred[192,3072]{1,0:T(8,128)(4,1)S(1)} %iota_compare_fusion), kind=kLoop, calls=%fused_computation.4 | loop fusion | flops 23591424 | bytes 19476480 | tf_op jit(solution)/shard_map/cond/branch_1_fun/reduce_sum | solution.py:68
  192.2 1.5 convolution_convert_fusion.3
  194.4 0.5 all-gather.12.cloned.1.call-update
  195.6 7.7 %reduce-scatter.3.cloned.1.call-done = bf16[96,2048]{1,0:T(8,128)(2,1)} async-done(((bf16[192,2048]{1,0:T(8,128)(2,1)}), bf16[96,2048]{1,0:T(8,128)(2,1)}) %reduce-scatter.3.cloned.1.call-update) | async-done | bytes 393232 | tf_op jit(solution)/shard_map/reduce_scatter | solution.py:92
  203.3 1.2 fusion.20
  204.6 1.2 fusion.22
  205.7 2.4 all_gather.20
  208.1 136.2 %all-gather.10.cloned.1.call-done = bf16[2048,2816]{1,0:T(8,128)(2,1)} async-done(((bf16[128,2816]{1,0:T(8,128)(2,1)}), bf16[2048,2816]{1,0:T(8,128)(2,1)}) %all-gather.10.cloned.1.call-update) | async-done | bytes 11534352 | tf_op jit(solution)/shard_map/all_gather | solution.py:102
  344.3 6.7 convolution_convert_fusion.1
  351.0 5.2 collective-permute-start
  356.3 130.2 %all-gather.12.cloned.1.call-done = bf16[2048,2816]{1,0:T(8,128)(2,1)} async-done(((bf16[128,2816]{1,0:T(8,128)(2,1)}), bf16[2048,2816]{1,0:T(8,128)(2,1)}) %all-gather.12.cloned.1.call-update) | async-done | bytes 11534352 | tf_op jit(solution)/shard_map/all_gather | solution.py:107
  486.5 182.8 %all-gather.14.cloned.1.call-done = bf16[2816,2048]{1,0:T(8,128)(2,1)} async-done(((bf16[2816,128]{1,0:T(8,128)(2,1)}), bf16[2816,2048]{1,0:T(8,128)(2,1)}) %all-gather.14.cloned.1.call-update) | async-done | bytes 11534352 | tf_op jit(solution)/shard_map/all_gather | solution.py:121
  669.3 15.2 %convolution_convert_fusion.2 = bf16[192,2048]{1,0:T(8,128)(2,1)} fusion(bf16[2816,2048]{1,0:T(8,128)(2,1)} %all-gather.14.cloned.1.call-done, bf16[192,2048]{1,0:T(8,128)(2,1)} %copy-done.4, bf16[2048,2816]{1,0:T(8,128)(2,1)} %all-gather.12.cloned.1.call-done, bf16[192,2816]{1,0:T(8,128)(2,1)} %copy-done.10, bf16[2,2816]{1,0:T(2,128)(2,1)S(1)} %collective-permute-done, ...), kind=kOutput, calls=%fused_computation.19 | convolution fusion | flops 4442013696 | bytes 25779200 | tf_op jit(solution)/shard_map/dot_general | solution.py:123
  684.6 10.7 %reduce-scatter.5.cloned.1.call-done = bf16[96,2048]{1,0:T(8,128)(2,1)} async-done(((bf16[192,2048]{1,0:T(8,128)(2,1)}), bf16[96,2048]{1,0:T(8,128)(2,1)}) %reduce-scatter.5.cloned.1.call-update) | async-done | bytes 393232 | tf_op jit(solution)/shard_map/reduce_scatter | solution.py:122
  695.3 1.9 fusion.23
  (48 shorter events, 2.5 us)
Async XLA Ops:
  6.5 185.7 %copy-start = (bf16[512,2048]{1,0:T(8,128)(2,1)S(1)}, bf16[512,2048]{1,0:T(8,128)(2,1)}, u32[]{:S(2)}) copy-start(bf16[512,2048]{1,0:T(8,128)(2,1)} %param.21) | copy-start | bytes 6291460
  6.5 70.6 %all-gather.6.cloned.1.call-start = ((), (), s32[]{:S(2)}) async-start(), calls=%async_computation.2 | async-start | bytes 3342336 | tf_op jit(solution)/shard_map/all_gather | solution.py:53
  7.3 139.1 %all-gather.8.cloned.1.call-start = ((), (), s32[]{:S(2)}) async-start(), calls=%async_computation.3 | async-start | bytes 3342336 | tf_op jit(solution)/shard_map/all_gather | solution.py:54
  8.0 195.3 %reduce-scatter.3.cloned.1.call-start = ((), (), s32[]{:S(2)}) async-start(), calls=%async_computation.4 | async-start | bytes 1179648 | tf_op jit(solution)/shard_map/reduce_scatter | solution.py:92
  146.4 45.3 %copy-start.9 = (f32[4]{0:T(128)S(1)}, f32[4]{0:T(128)}, u32[]{:S(2)}) copy-start(f32[4]{0:T(128)} %param.19) | copy-start | bytes 52
  146.4 45.8 %copy-start.8 = (f32[512]{0:T(512)S(1)}, f32[512]{0:T(512)}, u32[]{:S(2)}) copy-start(f32[512]{0:T(512)} %param.20) | copy-start | bytes 6148
  146.8 4.8 copy-start.5
  192.2 11.1 %copy-start.2 = (bf16[96,2048]{1,0:T(8,128)(2,1)S(1)}, bf16[96,2048]{1,0:T(8,128)(2,1)}, u32[]{:S(2)}) copy-start(bf16[96,2048]{1,0:T(8,128)(2,1)} %param.15) | copy-start | bytes 1179652
  192.2 12.3 %copy-start.7 = (f32[2048]{0:T(1024)S(1)}, f32[2048]{0:T(1024)}, u32[]{:S(2)}) copy-start(f32[2048]{0:T(1024)} %param.22) | copy-start | bytes 24580
  193.8 150.5 %all-gather.10.cloned.1.call-start = ((), (), s32[]{:S(2)}) async-start(), calls=%async_computation.5 | async-start | bytes 12255232 | tf_op jit(solution)/shard_map/all_gather | solution.py:102
  194.4 292.1 %all-gather.12.cloned.1.call-start = ((), (), s32[]{:S(2)}) async-start(), calls=%async_computation.6 | async-start | bytes 12255232 | tf_op jit(solution)/shard_map/all_gather | solution.py:107
  195.0 474.4 %all-gather.14.cloned.1.call-start = ((), (), s32[]{:S(2)}) async-start(), calls=%async_computation.7 | async-start | bytes 12255232 | tf_op jit(solution)/shard_map/all_gather | solution.py:121
  195.5 499.7 %reduce-scatter.5.cloned.1.call-start = ((), (), s32[]{:S(2)}) async-start(), calls=%async_computation.8 | async-start | bytes 1179648 | tf_op jit(solution)/shard_map/reduce_scatter | solution.py:122
  208.1 142.9 %copy-start.4 = (bf16[192,2048]{1,0:T(8,128)(2,1)}, bf16[192,2048]{1,0:T(8,128)(2,1)S(1)}, u32[]{:S(2)}) copy-start(bf16[192,2048]{1,0:T(8,128)(2,1)S(1)} %all_gather.20) | copy-start | bytes 2359300
  208.1 148.1 %copy-start.6 = (f32[3,2816]{1,0:T(4,128)S(1)}, f32[3,2816]{1,0:T(4,128)}, u32[]{:S(2)}) copy-start(f32[3,2816]{1,0:T(4,128)} %param.25) | copy-start | bytes 101380
  208.1 461.2 %copy-start.11 = (f32[2816]{0:T(1024)S(1)}, f32[2816]{0:T(1024)}, u32[]{:S(2)}) copy-start(f32[2816]{0:T(1024)} %param.26) | copy-start | bytes 33796
  351.0 5.2 copy-start.10
  351.0 318.4 %collective-permute-start = (bf16[2,2816]{1,0:T(2,128)(2,1)S(1)}, bf16[2,2816]{1,0:T(2,128)(2,1)S(1)}, u32[]{:S(2)}, u32[]{:S(2)}) collective-permute-start(bf16[2,2816]{1,0:T(2,128)(2,1)S(1)} %slice.41), channel_id=1, source_target_pairs={{0,2},{2,4},{4,6},{6,8},{8,10},{10,12},{12,14},{14,16},{16,18},{18... | collective-permute-start | bytes 33800 | tf_op jit(solution)/shard_map/ppermute | solution.py:17
  669.3 25.9 %copy-start.3 = (bf16[96,2048]{1,0:T(8,128)(2,1)S(1)}, bf16[96,2048]{1,0:T(8,128)(2,1)}, u32[]{:S(2)}) copy-start(bf16[96,2048]{1,0:T(8,128)(2,1)} %reduce-scatter.3.cloned.1.call-done) | copy-start | bytes 1179652
  669.3 27.8 %copy-start.1 = (bf16[512,2048]{1,0:T(8,128)(2,1)S(1)}, bf16[512,2048]{1,0:T(8,128)(2,1)}, u32[]{:S(2)}) copy-start(bf16[512,2048]{1,0:T(8,128)(2,1)} %param.21) | copy-start | bytes 6291460
Sparse Core Ops, SparseCore 0:
  10.1 67.0 all-gather.5
  79.9 66.3 all-gather.7
  193.9 9.3 reduce-scatter.2
  205.9 138.2 all-gather.9
  346.9 139.5 all-gather.11
  489.1 180.2 all-gather.13
  684.7 10.5 reduce-scatter.4
where the time goes:
time: 706 us; the launch traced here: 704 us
  waiting for transfers between devices  609 us (86%)
  matrix products  45.9 us (7%)
  other arithmetic  17.1 us (2%)
  between operations  13.7 us (2%)
  local copies, waits for them, and re-layouts  10.6 us (2%)
    all_gather x1, waiting for transfers between devices, local(): down_all = lax.all_gather(down_weight, 'sp', axis=1, tiled=True)  183 us
    all_gather x1, waiting for transfers between devices, local(): lax.all_gather(up_weight, 'sp', axis=0, tiled=True)  136 us
    all_gather x1, waiting for transfers between devices, local(): lax.all_gather(gate_weight, 'sp', axis=0, tiled=True)  130 us
    all_gather x1, waiting for transfers between devices, local(): value_piece = lax.all_gather(values, 'sp', axis=0, tiled=True)  69.2 us
    all_gather x1, waiting for transfers between devices, local(): key_piece = lax.all_gather(key_pairs, 'sp', axis=0, tiled=True)  69.1 us
    dot_general x1, matrix products, local(): jnp.dot(hidden, down_all, preferred_element_type=jnp.float32)  15.2 us
  transfers between devices with their start and end apart: 8, of which 7 were waited for; matrix products, arithmetic and copies ran while one was open for 1% of the time, Pallas kernels for 0%

commit v1 on v0

--- a/solution.py
+++ b/solution.py
@@ -1,7 +1,14 @@
+import functools
+
 import jax
 import jax.numpy as jnp
 from jax import lax
+from jax.experimental import pallas as pl
+from jax.experimental.pallas import tpu as pltpu
 from jax.sharding import PartitionSpec as P
+
+MESH = pl.DeviceIdType.MESH
+VMEM_LIMIT = 60 * 1024 * 1024
 
 HD = 64
 VD = 128
@@ -23,24 +30,9 @@
     return (values_f * scale_inv * gain).astype(jnp.bfloat16)
 
 
-def local(
-    residual,
-    queries,
-    key_pairs,
-    values,
-    second_weight,
-    head_gain,
-    out_weight,
-    norm_gain,
-    up_weight,
-    gate_weight,
-    conv_weight,
-    conv_bias,
-    down_weight,
-):
+def attend(queries, key_pairs, values, second_weight, head_gain):
     tok_rows = queries.shape[0]
     head_count = second_weight.shape[0]
-    ff_local = up_weight.shape[1]
     sp_index = lax.axis_index("sp")
     query = queries.reshape(tok_rows, head_count, 2, HD)
     query_pos = sp_index * tok_rows + jnp.arange(tok_rows)
@@ -89,6 +81,27 @@
         .reshape(tok_rows, head_count * VD)
         .astype(jnp.bfloat16)
     )
+    return attended
+
+
+def local(
+    residual,
+    queries,
+    key_pairs,
+    values,
+    second_weight,
+    head_gain,
+    out_weight,
+    norm_gain,
+    up_weight,
+    gate_weight,
+    conv_weight,
+    conv_bias,
+    down_weight,
+):
+    tok_rows = queries.shape[0]
+    ff_local = up_weight.shape[1]
+    attended = attend(queries, key_pairs, values, second_weight, head_gain)
     proj = lax.psum_scatter(
         jnp.dot(attended, out_weight, preferred_element_type=jnp.float32).astype(jnp.bfloat16),
         "tp",
@@ -128,9 +141,279 @@
     return (mid.astype(jnp.float32) + ffn_out.astype(jnp.float32)).astype(jnp.bfloat16)
 
 
+def greet(n, me, t):
+    barrier = pltpu.get_barrier_semaphore()
+
+    def signal(k, carry):
+        pl.semaphore_signal(
+            barrier, inc=1, device_id={"sp": lax.rem(me + k, n)}, device_id_type=MESH
+        )
+        return carry
+
+    lax.fori_loop(1, n, signal, 0)
+    pl.semaphore_signal(barrier, inc=1, device_id={"tp": 1 - t}, device_id_type=MESH)
+    pl.semaphore_wait(barrier, n)
+
+
+def to_sp(src, dst, send, recv, dest):
+    return pltpu.make_async_remote_copy(
+        src_ref=src, dst_ref=dst, send_sem=send, recv_sem=recv,
+        device_id={"sp": dest}, device_id_type=MESH,
+    )
+
+
+def to_tp(src, dst, send, recv, dest):
+    return pltpu.make_async_remote_copy(
+        src_ref=src, dst_ref=dst, send_sem=send, recv_sem=recv,
+        device_id={"tp": dest}, device_id_type=MESH,
+    )
+
+
+def gather_kernel(
+    n, att, ow, res, gain, wu, wg, up, gate, mid,
+    buf, pbuf, prbuf, psem, send, recv, fsend, frecv,
+):
+    me = lax.axis_index("sp")
+    t = lax.axis_index("tp")
+    half = res.shape[0]
+    rows = 2 * half
+    mine = pl.ds(pl.multiple_of(t * half, half), half)
+    theirs = pl.ds(pl.multiple_of((1 - t) * half, half), half)
+    greet(n, me, t)
+    pbuf[...] = jnp.dot(att[theirs, :], ow[...], preferred_element_type=jnp.float32).astype(
+        jnp.bfloat16
+    )
+    swap = to_tp(pbuf, prbuf, psem.at[0], psem.at[1], 1 - t)
+    swap.start()
+    own = jnp.dot(att[mine, :], ow[...], preferred_element_type=jnp.float32).astype(jnp.bfloat16)
+    swap.wait()
+    proj = (own.astype(jnp.float32) + prbuf[...].astype(jnp.float32)).astype(jnp.bfloat16)
+    mid_v = (res[...].astype(jnp.float32) + proj.astype(jnp.float32)).astype(jnp.bfloat16)
+    mid[...] = mid_v
+    mid_f = mid_v.astype(jnp.float32)
+    inv = lax.rsqrt(jnp.mean(mid_f * mid_f, axis=-1, keepdims=True) + eps)
+    buf[0, mine, :] = (mid_f * inv * gain[...]).astype(jnp.bfloat16)
+
+    def spread(k):
+        return to_sp(
+            buf.at[0, mine], buf.at[k, mine], send.at[k], recv.at[k], lax.rem(me + k, n)
+        )
+
+    def forward(k):
+        return to_tp(buf.at[k, mine], buf.at[k, mine], fsend.at[k], frecv.at[k], 1 - t)
+
+    def arrived(k):
+        return to_tp(buf.at[k, theirs], buf.at[k, theirs], fsend.at[k], frecv.at[k], 1 - t)
+
+    forward(0).start()
+
+    def start(k, carry):
+        spread(k).start()
+        return carry
+
+    lax.fori_loop(1, n, start, 0)
+
+    def compute(k):
+        arrived(k).wait_recv()
+        first = pl.multiple_of(lax.rem(me - k + n, n) * rows, rows)
+        block = buf[k]
+        up[pl.ds(first, rows), :] = jnp.dot(
+            block, wu[...], preferred_element_type=jnp.float32
+        ).astype(jnp.bfloat16)
+        gate[pl.ds(first, rows), :] = jnp.dot(
+            block, wg[...], preferred_element_type=jnp.float32
+        ).astype(jnp.bfloat16)
+
+    def step(k, carry):
+        spread(k).wait_recv()
+        forward(k).start()
+        compute(k - 1)
+        return carry
+
+    lax.fori_loop(1, n, step, 0)
+    compute(n - 1)
+
+    def drain(k, carry):
+        spread(k).wait_send()
+        forward(k).wait_send()
+        return carry
+
+    forward(0).wait_send()
+    lax.fori_loop(1, n, drain, 0)
+
+
+def scatter_kernel(
+    n, hid, down, mid, out, pb, pr, sb, rb, psend, precv, send, recv,
+):
+    me = lax.axis_index("sp")
+    t = lax.axis_index("tp")
+    half = mid.shape[0]
+    rows = 2 * half
+    greet(n, me, t)
+
+    def swap(k):
+        return to_tp(pb.at[k], pr.at[k], psend.at[k], precv.at[k], 1 - t)
+
+    def away(k):
+        return to_sp(sb.at[k], rb.at[k], send.at[k], recv.at[k], lax.rem(me + k, n))
+
+    def product(k):
+        first = lax.rem(me + k, n) * rows
+        theirs = pl.ds(pl.multiple_of(first + (1 - t) * half, half), half)
+        mine = pl.ds(pl.multiple_of(first + t * half, half), half)
+        pb[k] = jnp.dot(hid[theirs, :], down[...], preferred_element_type=jnp.float32).astype(
+            jnp.bfloat16
+        )
+        swap(k).start()
+        sb[k] = jnp.dot(hid[mine, :], down[...], preferred_element_type=jnp.float32).astype(
+            jnp.bfloat16
+        )
+
+    def combine(k):
+        swap(k).wait_recv()
+        sb[k] = (sb[k].astype(jnp.float32) + pr[k].astype(jnp.float32)).astype(jnp.bfloat16)
+
+    product(1)
+
+    def step(k, carry):
+        product(k)
+        combine(k - 1)
+        away(k - 1).start()
+        return carry
+
+    lax.fori_loop(2, n, step, 0)
+    product(0)
+    combine(n - 1)
+    away(n - 1).start()
+    combine(0)
+
+    total = sb[0].astype(jnp.float32)
+
+    def add(k, total):
+        away(k).wait_recv()
+        return total + rb[k].astype(jnp.float32)
+
+    acc = lax.fori_loop(1, n, add, total)
+    ffn = acc.astype(jnp.bfloat16).astype(jnp.float32)
+    out[...] = (mid[...].astype(jnp.float32) + ffn).astype(jnp.bfloat16)
+
+    def drain(k, carry):
+        away(k).wait_send()
+        swap(k).wait_send()
+        return carry
+
+    swap(0).wait_send()
+    lax.fori_loop(1, n, drain, 0)
+
+
+def vm(count):
+    return [pl.BlockSpec(memory_space=pltpu.VMEM)] * count
+
+
+def params(cid):
+    return pltpu.CompilerParams(
+        collective_id=cid, has_side_effects=True, vmem_limit_bytes=VMEM_LIMIT
+    )
+
+
+def gather_rows(n, att, ow, res, gain, wu, wg):
+    half, width = res.shape
+    units = wu.shape[1]
+    rows = 2 * half
+    bf = jnp.bfloat16
+    dma = pltpu.SemaphoreType.DMA
+    return pl.pallas_call(
+        functools.partial(gather_kernel, n),
+        out_shape=(
+            jax.ShapeDtypeStruct((n * rows, units), bf),
+            jax.ShapeDtypeStruct((n * rows, units), bf),
+            jax.ShapeDtypeStruct((half, width), bf),
+        ),
+        in_specs=vm(6),
+        out_specs=tuple(vm(3)),
+        scratch_shapes=[
+            pltpu.VMEM((n, rows, width), bf),
+            pltpu.VMEM((half, width), bf),
+            pltpu.VMEM((half, width), bf),
+            dma((2,)), dma((n,)), dma((n,)), dma((n,)), dma((n,)),
+        ],
+        compiler_params=params(1),
+        name="gather_rows",
+    )(att, ow, res, gain[None, :], wu, wg)
+
+
+def scatter_rows(n, hid, down, mid):
+    half, width = mid.shape
+    bf = jnp.bfloat16
+    dma = pltpu.SemaphoreType.DMA
+    block = pltpu.VMEM((n, half, width), bf)
+    return pl.pallas_call(
+        functools.partial(scatter_kernel, n),
+        out_shape=jax.ShapeDtypeStruct((half, width), bf),
+        in_specs=vm(3),
+        out_specs=vm(1)[0],
+        scratch_shapes=[block, block, block, block, dma((n,)), dma((n,)), dma((n,)), dma((n,))],
+        compiler_params=params(2),
+        name="scatter_rows",
+    )(hid, down, mid)
+
+
+def moving_rows(
+    n,
+    residual,
+    queries,
+    key_pairs,
+    values,
+    second_weight,
+    head_gain,
+    out_weight,
+    norm_gain,
+    up_weight,
+    gate_weight,
+    conv_weight,
+    conv_bias,
+    down_weight,
+):
+    sp_index = lax.axis_index("sp")
+    units = up_weight.shape[1] // n
+    taps = conv_weight.shape[0]
+    wu = lax.all_to_all(up_weight, "sp", split_axis=1, concat_axis=0, tiled=True)
+    wg = lax.all_to_all(gate_weight, "sp", split_axis=1, concat_axis=0, tiled=True)
+    wd = lax.all_to_all(down_weight, "sp", split_axis=0, concat_axis=1, tiled=True)
+    cw = lax.dynamic_slice_in_dim(conv_weight, sp_index * units, units, 1)
+    cb = lax.dynamic_slice_in_dim(conv_bias, sp_index * units, units, 0)
+    attended = attend(queries, key_pairs, values, second_weight, head_gain)
+    up, gate, mid = gather_rows(n, attended, out_weight, residual, norm_gain, wu, wg)
+    count = up.shape[0]
+    extended = jnp.pad(up, ((taps - 1, 0), (0, 0)))
+    conv_out = jnp.zeros((count, units), jnp.float32) + cb[None, :]
+    for tap in range(taps):
+        conv_out = conv_out + cw[tap][None, :] * extended[tap : tap + count].astype(jnp.float32)
+    hidden = (jax.nn.silu(conv_out) * gate.astype(jnp.float32)).astype(jnp.bfloat16)
+    return scatter_rows(n, hidden, wd, mid)
+
+
+def choose(n_sp, n_tp):
+    def body(residual, queries, *rest):
+        up_weight = rest[6]
+        token_count = queries.shape[0] * n_sp
+        width = residual.shape[1]
+        moves_rows = (
+            n_tp == 2
+            and 2 * token_count < 3 * n_tp * up_weight.shape[1]
+            and up_weight.shape[1] % n_sp == 0
+            and n_sp % rest[2].shape[0] == 0
+        )
+        if moves_rows:
+            return moving_rows(n_sp, residual, queries, *rest)
+        return local(residual, queries, *rest)
+
+    return body
+
+
 def solution(mesh):
     return jax.shard_map(
-        local,
+        choose(mesh.shape["sp"], mesh.shape["tp"]),
         mesh=mesh,
         in_specs=(
             P(("sp", "tp"), None),

time: 706 us -> 585 us (0.83)
  waiting for transfers between devices: 609 us -> 113 us
  Pallas kernels: 0 us -> 356 us
  blocking collectives: 2.37 us -> 28.6 us
  matrix products: 45.9 us -> 22.5 us
  local copies, waits for them, and re-layouts: 10.6 us -> 20 us
    all_gather x5 -> x2, waiting for transfers between devices: 587 us -> 65.9 us  [the longest x1 65.9 us: attend(): value_piece = lax.all_gather(values, 'sp', axis=0, tiled=True)]
    pallas_call x0 -> x2, Pallas kernels: none -> 356 us  [the longest x1 184 us: gather_rows(): pl.pallas_call(functools.partial(gather_kernel, n), out_shape=(jax.ShapeD...]
    all_to_all x0 -> x2, waiting for transfers between devices: none -> 45.5 us  [the longest x1 24.9 us: moving_rows(): lax.all_to_all(down_weight, 'sp', split_axis=0, concat_axis=1, tiled=True)]
    all_to_all x0 -> x1, blocking collectives: none -> 28.6 us  [moving_rows(): lax.all_to_all(gate_weight, 'sp', split_axis=1, concat_axis=0, tiled=True)]
    dot_general x3 -> x0, matrix products: 23.4 us -> none  [the longest x1 15.2 us: local(): jnp.dot(hidden, down_all, preferred_element_type=jnp.float32)]
    reduce_scatter x2 -> x0, waiting for transfers between devices: 18.4 us -> none  [the longest x1 10.7 us: local(): lax.psum_scatter(jnp.dot(hidden, down_all, preferred_element_type=jnp.flo...]
    all_to_all x0 -> x2, starting transfers between devices: none -> 12.1 us  [the longest x1 6.58 us: moving_rows(): lax.all_to_all(up_weight, 'sp', split_axis=1, concat_axis=0, tiled=True)]
  transfers between devices with their start and end apart: 8 -> 4, of which waited for: 7 -> 3; matrix products, arithmetic and copies ran while one was open for 1% -> 1% of each run, Pallas kernels for 0% -> 0%
where the time goes in v1:
time: 585 us; the launch traced here: 584 us
  Pallas kernels  356 us (61%)
  waiting for transfers between devices  113 us (19%)
  blocking collectives  28.6 us (5%)
  matrix products  22.5 us (4%)
  local copies, waits for them, and re-layouts  20 us (3%)
  other arithmetic  19 us (3%)
  between operations  13.5 us (2%)
  starting transfers between devices  12.1 us (2%)
    pallas_call x1, Pallas kernels, gather_rows(): pl.pallas_call(functools.partial(gather_kernel, n), out_shape=(jax.ShapeD...  184 us
    pallas_call x1, Pallas kernels, scatter_rows(): pl.pallas_call(functools.partial(scatter_kernel, n), out_shape=jax.ShapeD...  172 us
    all_gather x1, waiting for transfers between devices, attend(): value_piece = lax.all_gather(values, 'sp', axis=0, tiled=True)  65.9 us
    all_to_all x1, blocking collectives, moving_rows(): lax.all_to_all(gate_weight, 'sp', split_axis=1, concat_axis=0, tiled=True)  28.6 us
    all_to_all x1, waiting for transfers between devices, moving_rows(): lax.all_to_all(down_weight, 'sp', split_axis=0, concat_axis=1, tiled=True)  24.9 us
    all_to_all x1, waiting for transfers between devices, moving_rows(): lax.all_to_all(up_weight, 'sp', split_axis=1, concat_axis=0, tiled=True)  20.7 us
    reduce_sum x1, other arithmetic, compute(): totals = jnp.sum(exp_scores, axis=-1)  11.9 us
    dot_general x1, matrix products, compute(): jnp.einsum('qhmd,khmd->hmqk', query, key_rows, preferred_element_type=jnp...  11.8 us
  transfers between devices with their start and end apart: 4, of which 3 were waited for; matrix products, arithmetic and copies ran while one was open for 1% of the time, Pallas kernels for 0%

profile of v1, /device:TPU:15, one launch (start us, length us, event | category | flops | bytes accessed | tf_op | source)
XLA Modules:
  0.0 584.3 jit_solution(2376842521158096506)
XLA Ops:
  6.5 0.7 all-gather.3.cloned.1.call-update
  8.0 2.2 copy.38
  10.3 6.6 %all-to-all-start = ((bf16[128,16,176]{0,2,1:T(8,128)(2,1)}), bf16[128,16,176]{0,2,1:T(8,128)(2,1)S(1)}, u32[]{:S(2)}, u32[]{:S(2)}) async-start(bf16[128,16,176]{0,2,1:T(8,128)(2,1)} %bitcast.9), calls=%async_computation | async-start | bytes 1441792 | tf_op jit(solution)/shard_map/all_to_all | solution.py:380
  17.2 20.7 %all-to-all-done = bf16[128,16,176]{0,2,1:T(8,128)(2,1)S(1)} async-done(((bf16[128,16,176]{0,2,1:T(8,128)(2,1)}), bf16[128,16,176]{0,2,1:T(8,128)(2,1)S(1)}, u32[]{:S(2)}, u32[]{:S(2)}) %all-to-all-start) | async-done | bytes 720928 | tf_op jit(solution)/shard_map/all_to_all | solution.py:380
  37.9 28.6 %all_to_all.57 = bf16[128,16,176]{0,2,1:T(8,128)(2,1)S(1)} all-to-all(bf16[128,16,176]{0,2,1:T(8,128)(2,1)S(1)} %bitcast.57), channel_id=1, replica_groups=mesh['sp'=16,'tp'=2] {'sp'}, dimensions={1} | all-to-all | bytes 1441792 | tf_op jit(solution)/shard_map/all_to_all | solution.py:381
  66.5 5.5 all-to-all-start.2
  72.1 0.8 dynamic_slice.6
  72.8 0.9 constant_dynamic-slice_fusion
  73.7 1.3 copy.39
  75.0 1.3 copy.41
  76.3 24.9 %all-to-all-done.2 = bf16[16,176,128]{2,1,0:T(8,128)(2,1)S(1)} async-done(((bf16[16,176,128]{2,1,0:T(8,128)(2,1)}), bf16[16,176,128]{2,1,0:T(8,128)(2,1)S(1)}, u32[]{:S(2)}, u32[]{:S(2)}) %all-to-all-start.2) | async-done | bytes 720928 | tf_op jit(solution)/shard_map/all_to_all | solution.py:382
  101.2 1.0 copy_bitcast_fusion.down
  102.1 65.9 %all-gather.5.cloned.1.call-done = bf16[3072,512]{1,0:T(8,128)(2,1)} async-done(((bf16[192,512]{1,0:T(8,128)(2,1)}), bf16[3072,512]{1,0:T(8,128)(2,1)}) %all-gather.5.cloned.1.call-update) | async-done | bytes 3145744 | tf_op jit(solution)/shard_map/all_gather | solution.py:46
  168.0 45.2 %conditional.1 = (f32[4,2,192]{2,1,0:T(2,128)S(1)}, f32[4,2,192,128]{3,2,1,0:T(8,128)S(1)}) conditional(s32[]{:T(128)} %convert_element_type.28, () %tuple.13, (s32[]{:T(128)}, s32[192]{0:T(256)S(1)}, bf16[192,512]{1,0:T(8,128)(2,1)S(1)}, bf16[3072,512]{1,0:T(8,128)(2,1)}, bf16[3072,512]{1,0:T(8,128)(2,1)}) %tuple.30), branch_computations={%region_0.0_spmd, %region_1.4_spmd} | conditional | flops 1873869568 | bytes 79272224 | solution.py:72
  168.4 4.7 copy.35
  173.3 11.8 %fusion = (f32[4,2,192]{2,1,0:T(2,128)S(1)}, f32[4,2,192,3072]{3,2,1,0:T(8,128)}) fusion(pred[192,3072]{1,0:T(8,128)(4,1)S(1)} %iota_compare_fusion, bf16[192,4,2,64]{0,3,2,1:T(8,128)(2,1)S(1)} %bitcast.58, bf16[3072,4,2,64]{0,3,2,1:T(8,128)(2,1)} %bitcast.51), kind=kOutput, calls=%fused_computation.2 | convolution fusion | flops 618134016 | bytes 22812672 | tf_op jit(solution)/shard_map/cond/branch_1_fun/qhmd,khmd->hmqk/dot_general | solution.py:53
  185.1 5.5 reshape.37
  190.6 10.7 %fusion.3 = f32[4,2,192,128]{3,2,1,0:T(8,128)S(1)} fusion(f32[4,2,192,3072]{3,2,1,0:T(8,128)} %get-tuple-element.55, f32[4,2,192]{2,1,0:T(2,128)S(1)} %broadcast_maximum_fusion, pred[192,3072]{1,0:T(8,128)(4,1)S(1)} %iota_compare_fusion, bf16[3072,4,128,1]{2,1,0,3:T(4,128)(2,1)} %bitcast.54), kind=kOutput, calls=%fused_computation.5 | convolution fusion | flops 1231552512 | bytes 23402496 | tf_op jit(solution)/shard_map/cond/branch_1_fun/hmqk,khe->hmqe/dot_general | solution.py:61
  201.3 11.9 %fusion.2 = f32[4,2,192]{2,1,0:T(2,128)S(1)} fusion(f32[4,2,192,3072]{3,2,1,0:T(8,128)} %get-tuple-element.55, f32[4,2,192]{2,1,0:T(2,128)S(1)} %broadcast_maximum_fusion, pred[192,3072]{1,0:T(8,128)(4,1)S(1)} %iota_compare_fusion), kind=kLoop, calls=%fused_computation.4 | loop fusion | flops 23591424 | bytes 19476480 | tf_op jit(solution)/shard_map/cond/branch_1_fun/reduce_sum | solution.py:60
  213.8 0.9 copy_bitcast_fusion.1.att
  214.6 183.8 %gather_rows.1 = (bf16[3072,176]{1,0:T(8,128)(2,1)}, bf16[3072,176]{1,0:T(8,128)(2,1)}, bf16[96,2048]{1,0:T(8,128)(2,1)}) custom-call(bf16[192,512]{1,0:T(8,128)(2,1)} %copy_bitcast_fusion.1.att, bf16[512,2048]{1,0:T(8,128)(2,1)} %ow.1, bf16[96,2048]{1,0:T(8,128)(2,1)} %res.1, f32[1,2048]{1,0:T(1,128)} %bitcast.59, bf16[2048,176]{1,0:T(8,128)(2,1)} %bitcast.52, ...), custom_call_target="tpu_custom_call" | custom-call | tf_op jit(solution)/shard_map/gather_rows/pallas_call | solution.py:325
  398.5 5.4 multiply_convert_fusion.hid
  403.8 171.8 %scatter_rows.1 = bf16[96,2048]{1,0:T(8,128)(2,1)} custom-call(bf16[3072,176]{1,0:T(8,128)(2,1)} %multiply_convert_fusion.hid, bf16[176,2048]{1,0:T(8,128)(2,1)} %copy_bitcast_fusion.down, bf16[96,2048]{1,0:T(8,128)(2,1)} %get-tuple-element.34.mid), custom_call_target="tpu_custom_call" | custom-call | tf_op jit(solution)/shard_map/scatter_rows/pallas_call | solution.py:350
  575.7 1.8 copy.63
  (22 shorter events, 2.1 us)
Async XLA Ops:
  6.5 10.3 %copy-start = (bf16[128,2816]{1,0:T(8,128)(2,1)S(1)}, bf16[128,2816]{1,0:T(8,128)(2,1)}, u32[]{:S(2)}) copy-start(bf16[128,2816]{1,0:T(8,128)(2,1)} %param.24) | copy-start | bytes 2162692
  6.5 95.6 %all-gather.3.cloned.1.call-start = ((), (), s32[]{:S(2)}) async-start(), calls=%async_computation.3 | async-start | bytes 3342336 | tf_op jit(solution)/shard_map/all_gather | solution.py:45
  7.3 160.8 %all-gather.5.cloned.1.call-start = ((), (), s32[]{:S(2)}) async-start(), calls=%async_computation.4 | async-start | bytes 3342336 | tf_op jit(solution)/shard_map/all_gather | solution.py:46
  10.3 27.6 %all-to-all-start = ((bf16[128,16,176]{0,2,1:T(8,128)(2,1)}), bf16[128,16,176]{0,2,1:T(8,128)(2,1)S(1)}, u32[]{:S(2)}, u32[]{:S(2)}) async-start(bf16[128,16,176]{0,2,1:T(8,128)(2,1)} %bitcast.9), calls=%async_computation | async-start | bytes 1441792 | tf_op jit(solution)/shard_map/all_to_all | solution.py:380
  66.5 101.5 %copy-start.1 = (bf16[192,512]{1,0:T(8,128)(2,1)S(1)}, bf16[192,512]{1,0:T(8,128)(2,1)}, u32[]{:S(2)}) copy-start(bf16[192,512]{1,0:T(8,128)(2,1)} %param.16) | copy-start | bytes 589828
  66.5 34.7 %all-to-all-start.2 = ((bf16[16,176,128]{2,1,0:T(8,128)(2,1)}), bf16[16,176,128]{2,1,0:T(8,128)(2,1)S(1)}, u32[]{:S(2)}, u32[]{:S(2)}) async-start(bf16[16,176,128]{2,1,0:T(8,128)(2,1)} %bitcast.17), calls=%async_computation.2 | async-start | bytes 1441792 | tf_op jit(solution)/shard_map/all_to_all | solution.py:382
  168.0 45.2 %copy-start.3 = (f32[4]{0:T(128)S(1)}, f32[4]{0:T(128)}, u32[]{:S(2)}) copy-start(f32[4]{0:T(128)} %param.19) | copy-start | bytes 52
  168.0 45.8 %copy-start.2 = (f32[512]{0:T(512)S(1)}, f32[512]{0:T(512)}, u32[]{:S(2)}) copy-start(f32[512]{0:T(512)} %param.20) | copy-start | bytes 6148
Sparse Core Ops, SparseCore 0:
  10.1 87.0 all-gather.2
  100.0 68.0 all-gather.4

commit v2 on v1

--- a/solution.py
+++ b/solution.py
@@ -1,4 +1,5 @@
 import functools
+import math
 
 import jax
 import jax.numpy as jnp
@@ -194,9 +195,19 @@
     inv = lax.rsqrt(jnp.mean(mid_f * mid_f, axis=-1, keepdims=True) + eps)
     buf[0, mine, :] = (mid_f * inv * gain[...]).astype(jnp.bfloat16)
 
-    def spread(k):
+    p = plane_of(n)
+    layers = n // p
+    z, w = me // p, lax.rem(me, p)
+
+    def column(a):
+        dest = lax.rem(z + a, layers) * p + w
+        return to_sp(buf.at[0, mine], buf.at[a * p, mine], send.at[a * p], recv.at[a * p], dest)
+
+    def spread(a, b):
+        slot = a * p + b
+        dest = z * p + lax.rem(w + b, p)
         return to_sp(
-            buf.at[0, mine], buf.at[k, mine], send.at[k], recv.at[k], lax.rem(me + k, n)
+            buf.at[a * p, mine], buf.at[slot, mine], send.at[slot], recv.at[slot], dest
         )
 
     def forward(k):
@@ -205,18 +216,16 @@
     def arrived(k):
         return to_tp(buf.at[k, theirs], buf.at[k, theirs], fsend.at[k], frecv.at[k], 1 - t)
 
-    forward(0).start()
-
-    def start(k, carry):
-        spread(k).start()
-        return carry
-
-    lax.fori_loop(1, n, start, 0)
-
-    def compute(k):
-        arrived(k).wait_recv()
-        first = pl.multiple_of(lax.rem(me - k + n, n) * rows, rows)
-        block = buf[k]
+    def relay(a):
+        for b in range(1, p):
+            spread(a, b).start()
+        forward(a * p).start()
+
+    def compute(a, b):
+        arrived(a * p + b).wait_recv()
+        source = lax.rem(z - a + layers, layers) * p + lax.rem(w - b + p, p)
+        first = pl.multiple_of(source * rows, rows)
+        block = buf[a * p + b]
         up[pl.ds(first, rows), :] = jnp.dot(
             block, wu[...], preferred_element_type=jnp.float32
         ).astype(jnp.bfloat16)
@@ -224,86 +233,139 @@
             block, wg[...], preferred_element_type=jnp.float32
         ).astype(jnp.bfloat16)
 
-    def step(k, carry):
-        spread(k).wait_recv()
-        forward(k).start()
-        compute(k - 1)
+    for a in range(1, layers):
+        column(a).start()
+    relay(0)
+
+    def stage(a, carry):
+        @pl.when(a + 1 < layers)
+        def _():
+            column(a + 1).wait_recv()
+            relay(a + 1)
+
+        def step(b, carry):
+            spread(a, b).wait_recv()
+            forward(a * p + b).start()
+            compute(a, b - 1)
+            return carry
+
+        lax.fori_loop(1, p, step, 0)
+        compute(a, p - 1)
         return carry
 
-    lax.fori_loop(1, n, step, 0)
-    compute(n - 1)
-
-    def drain(k, carry):
-        spread(k).wait_send()
-        forward(k).wait_send()
+    lax.fori_loop(0, layers, stage, 0)
+
+    def drain(a, carry):
+        for b in range(1, p):
+            spread(a, b).wait_send()
+            forward(a * p + b).wait_send()
+        forward(a * p).wait_send()
         return carry
 
-    forward(0).wait_send()
-    lax.fori_loop(1, n, drain, 0)
+    lax.fori_loop(0, layers, drain, 0)
+    for a in range(1, layers):
+        column(a).wait_send()
 
 
 def scatter_kernel(
-    n, hid, down, mid, out, pb, pr, sb, rb, psend, precv, send, recv,
+    n, hid, down, mid, out, pb, pr, sb, rb, zb, cb, psend, precv, send, recv, zsend, zrecv,
 ):
     me = lax.axis_index("sp")
     t = lax.axis_index("tp")
     half = mid.shape[0]
     rows = 2 * half
+    p = plane_of(n)
+    layers = n // p
+    z, w = me // p, lax.rem(me, p)
     greet(n, me, t)
 
-    def swap(k):
-        return to_tp(pb.at[k], pr.at[k], psend.at[k], precv.at[k], 1 - t)
-
-    def away(k):
-        return to_sp(sb.at[k], rb.at[k], send.at[k], recv.at[k], lax.rem(me + k, n))
-
-    def product(k):
-        first = lax.rem(me + k, n) * rows
+    def place(i):
+        return lax.rem(i // p + 1, layers), lax.rem(lax.rem(i, p) + 1, p)
+
+    def swap(i):
+        a, b = place(i)
+        slot = a * p + b
+        return to_tp(pb.at[slot], pr.at[slot], psend.at[slot], precv.at[slot], 1 - t)
+
+    def across(a, b):
+        slot = a * p + b
+        dest = z * p + lax.rem(w + b, p)
+        return to_sp(sb.at[slot], rb.at[slot], send.at[slot], recv.at[slot], dest)
+
+    def column(a):
+        dest = lax.rem(z + a, layers) * p + w
+        return to_sp(zb.at[a], cb.at[a], zsend.at[a], zrecv.at[a], dest)
+
+    def product(i):
+        a, b = place(i)
+        slot = a * p + b
+        first = (lax.rem(z + a, layers) * p + lax.rem(w + b, p)) * rows
         theirs = pl.ds(pl.multiple_of(first + (1 - t) * half, half), half)
         mine = pl.ds(pl.multiple_of(first + t * half, half), half)
-        pb[k] = jnp.dot(hid[theirs, :], down[...], preferred_element_type=jnp.float32).astype(
+        pb[slot] = jnp.dot(hid[theirs, :], down[...], preferred_element_type=jnp.float32).astype(
             jnp.bfloat16
         )
-        swap(k).start()
-        sb[k] = jnp.dot(hid[mine, :], down[...], preferred_element_type=jnp.float32).astype(
+        swap(i).start()
+        sb[slot] = jnp.dot(hid[mine, :], down[...], preferred_element_type=jnp.float32).astype(
             jnp.bfloat16
         )
 
-    def combine(k):
-        swap(k).wait_recv()
-        sb[k] = (sb[k].astype(jnp.float32) + pr[k].astype(jnp.float32)).astype(jnp.bfloat16)
-
-    product(1)
-
-    def step(k, carry):
-        product(k)
-        combine(k - 1)
-        away(k - 1).start()
+    def combine(i):
+        a, b = place(i)
+        slot = a * p + b
+        swap(i).wait_recv()
+        sb[slot] = (sb[slot].astype(jnp.float32) + pr[slot].astype(jnp.float32)).astype(
+            jnp.bfloat16
+        )
+
+        @pl.when(b != 0)
+        def _():
+            across(a, b).start()
+
+    def plane_sum(a):
+        acc = sb[a * p].astype(jnp.float32)
+        for b in range(1, p):
+            across(a, b).wait_recv()
+            acc = acc + rb[a * p + b].astype(jnp.float32)
+        return acc
+
+    product(0)
+
+    def step(i, carry):
+        product(i)
+        combine(i - 1)
+
+        @pl.when(jnp.logical_and(lax.rem(i, p) == p - 1, i >= p))
+        def _():
+            a = i // p
+            zb[a] = plane_sum(a).astype(jnp.bfloat16)
+            column(a).start()
+
         return carry
 
-    lax.fori_loop(2, n, step, 0)
-    product(0)
+    lax.fori_loop(1, n, step, 0)
     combine(n - 1)
-    away(n - 1).start()
-    combine(0)
-
-    total = sb[0].astype(jnp.float32)
-
-    def add(k, total):
-        away(k).wait_recv()
-        return total + rb[k].astype(jnp.float32)
-
-    acc = lax.fori_loop(1, n, add, total)
+    acc = plane_sum(0)
+    for a in range(1, layers):
+        column(a).wait_recv()
+        acc = acc + cb[a].astype(jnp.float32)
     ffn = acc.astype(jnp.bfloat16).astype(jnp.float32)
     out[...] = (mid[...].astype(jnp.float32) + ffn).astype(jnp.bfloat16)
 
-    def drain(k, carry):
-        away(k).wait_send()
-        swap(k).wait_send()
+    def drain(a, carry):
+        for b in range(1, p):
+            across(a, b).wait_send()
+        for b in range(p):
+            swap(a * p + b).wait_send()
         return carry
 
-    swap(0).wait_send()
-    lax.fori_loop(1, n, drain, 0)
+    lax.fori_loop(0, layers, drain, 0)
+    for a in range(1, layers):
+        column(a).wait_send()
+
+
+def plane_of(n):
+    return math.gcd(n, 4)
 
 
 def vm(count):
@@ -346,16 +408,235 @@
     half, width = mid.shape
     bf = jnp.bfloat16
     dma = pltpu.SemaphoreType.DMA
+    layers = n // plane_of(n)
     block = pltpu.VMEM((n, half, width), bf)
+    few = pltpu.VMEM((layers, half, width), bf)
     return pl.pallas_call(
         functools.partial(scatter_kernel, n),
         out_shape=jax.ShapeDtypeStruct((half, width), bf),
         in_specs=vm(3),
         out_specs=vm(1)[0],
-        scratch_shapes=[block, block, block, block, dma((n,)), dma((n,)), dma((n,)), dma((n,))],
+        scratch_shapes=[block, block, block, block, few, few]
+        + [dma((n,)), dma((n,)), dma((n,)), dma((n,)), dma((layers,)), dma((layers,))],
         compiler_params=params(2),
         name="scatter_rows",
     )(hid, down, mid)
+
+
+def attention_kernel(
+    n, heads, q, k, v, sw, gain, ub, gb, db, att, wu, wg, wd,
+    qb, kb, vb, ob, qsend, qrecv, ksend, krecv, vsend, vrecv, osend, orecv,
+    usend, urecv, gsend, grecv, dsend, drecv,
+):
+    me = lax.axis_index("sp")
+    t = lax.axis_index("tp")
+    rows = q.shape[0]
+    depth = db.shape[2]
+    groups = n // heads
+    chunk = 2 * rows
+
+    def cols(h):
+        return pl.ds(pl.multiple_of(h * VD, VD), VD)
+
+    def at(s):
+        return pl.ds(pl.multiple_of(s * rows, rows), rows)
+
+    def group_of(s):
+        i, r = s // groups, lax.rem(s, groups)
+        return jnp.where(lax.rem(i, 2) == 0, r, groups - 1 - r)
+
+    head = lax.rem(me, heads)
+    group = me // heads
+    my_group = group_of(me)
+    my_slot = me // groups
+    greet(n, me, t)
+
+    def query_copy(h):
+        return to_sp(
+            q.at[:, cols(h)], qb.at[my_slot], qsend.at[h], qrecv.at[my_slot], my_group * heads + h
+        )
+
+    def block_of(i):
+        return i * groups + (group if i % 2 == 0 else groups - 1 - group)
+
+    def query_wait(i):
+        to_sp(qb.at[i], qb.at[i], qsend.at[0], qrecv.at[i], me).wait_recv()
+
+    for h in range(heads):
+        other = my_group * heads + h != me
+
+        @pl.when(other)
+        def _():
+            query_copy(h).start()
+
+        @pl.when(jnp.logical_not(other))
+        def _():
+            qb[my_slot] = q[:, cols(h)]
+
+    def pair(d):
+        dest = lax.rem(me + d, n)
+        h = lax.rem(dest, heads)
+        return (
+            to_sp(k.at[:, cols(h)], kb.at[at(me)], ksend.at[d], krecv.at[d], dest),
+            to_sp(v.at[:, cols(h)], vb.at[at(me)], vsend.at[d], vrecv.at[d], dest),
+        )
+
+    def weights(d):
+        dest = lax.rem(me + d, n)
+        wide = pl.ds(pl.multiple_of(me * depth, depth), depth)
+        return (
+            to_sp(ub.at[dest], wu.at[me], usend.at[d], urecv.at[d], dest),
+            to_sp(gb.at[dest], wg.at[me], gsend.at[d], grecv.at[d], dest),
+            to_sp(db.at[dest], wd.at[:, wide], dsend.at[d], drecv.at[d], dest),
+        )
+
+    def begin(make):
+        def start(d, carry):
+            for copy in make(d):
+                copy.start()
+            return carry
+
+        lax.fori_loop(1, n, start, 0)
+
+    def finish(make, sent):
+        def wait(d, carry):
+            for copy in make(d):
+                if sent:
+                    copy.wait_send()
+                else:
+                    copy.wait_recv()
+            return carry
+
+        lax.fori_loop(1, n, wait, 0)
+
+    begin(pair)
+    begin(weights)
+    kb[at(me), :] = k[:, cols(head)]
+    vb[at(me), :] = v[:, cols(head)]
+    wu[me] = ub[me]
+    wg[me] = gb[me]
+    wd[:, pl.ds(pl.multiple_of(me * depth, depth), depth)] = db[me]
+    for i in range(heads):
+
+        @pl.when(block_of(i) != me)
+        def _():
+            query_wait(i)
+
+    finish(pair, False)
+    weight = sw[head]
+    gain_row = gain[pl.ds(head, 1), :]
+    lane = lax.broadcasted_iota(jnp.int32, (rows, VD), 1)
+
+    def answer(i):
+        return to_sp(
+            ob.at[i], att.at[:, cols(head)], osend.at[i], orecv.at[head], block_of(i)
+        )
+
+    for i in range(heads):
+        block = block_of(i)
+        query = (qb[i].astype(jnp.float32) * HD ** (-0.5)).astype(jnp.bfloat16)
+        zero = jnp.zeros_like(query)
+        both = jnp.concatenate(
+            (jnp.where(lane < HD, query, zero), jnp.where(lane < HD, zero, query)), axis=0
+        )
+        last = block // 2
+
+        def visit(c, state, masked):
+            top, total, acc = state
+            span = pl.ds(pl.multiple_of(c * chunk, chunk), chunk)
+            scores = lax.dot_general(
+                both, kb[span, :], (((1,), (1,)), ((), ())), preferred_element_type=jnp.float32
+            )
+            if masked:
+                row = lax.broadcasted_iota(jnp.int32, scores.shape, 0)
+                row = jnp.where(row < rows, row, row - rows)
+                col = lax.broadcasted_iota(jnp.int32, scores.shape, 1)
+                visible = c * chunk + col <= block * rows + row
+                scores = jnp.where(visible, scores, neg_fill)
+            new_top = jnp.maximum(top, jnp.max(scores, axis=-1, keepdims=True))
+            shrink = jnp.exp(top - new_top)
+            exp_scores = jnp.exp(scores - new_top)
+            total = total * shrink + jnp.sum(exp_scores, axis=-1, keepdims=True)
+            acc = acc * shrink + jnp.dot(
+                exp_scores.astype(jnp.bfloat16), vb[span, :], preferred_element_type=jnp.float32
+            )
+            return new_top, total, acc
+
+        state = (
+            jnp.full((2 * rows, 1), neg_fill, jnp.float32),
+            jnp.zeros((2 * rows, 1), jnp.float32),
+            jnp.zeros((2 * rows, VD), jnp.float32),
+        )
+        state = lax.fori_loop(0, last, lambda c, state: visit(c, state, False), state)
+        top, total, acc = visit(last, state, True)
+        mean_v = acc / total
+        diff = mean_v[:rows] - weight * mean_v[rows:]
+        inv = lax.rsqrt(jnp.mean(diff * diff, axis=-1, keepdims=True) + eps)
+        result = (diff * inv * gain_row * 0.8).astype(jnp.bfloat16)
+
+        @pl.when(block != me)
+        def _():
+            ob[i] = result
+            answer(i).start()
+
+        @pl.when(block == me)
+        def _():
+            att[:, cols(head)] = result
+
+    for h in range(heads):
+        other = my_group * heads + h != me
+
+        @pl.when(other)
+        def _():
+            to_sp(ob.at[0], att.at[:, cols(h)], osend.at[0], orecv.at[h], me).wait_recv()
+            query_copy(h).wait_send()
+
+    for i in range(heads):
+
+        @pl.when(block_of(i) != me)
+        def _():
+            answer(i).wait_send()
+
+    finish(pair, True)
+    finish(weights, False)
+    finish(weights, True)
+
+
+def attend_rows(n, q, k, v, second_weight, head_gain, up_weight, gate_weight, down_weight):
+    rows, width = q.shape
+    heads = second_weight.shape[0]
+    depth, ff_local = up_weight.shape
+    units = ff_local // n
+    bf = jnp.bfloat16
+    dma = pltpu.SemaphoreType.DMA
+    ub = up_weight.reshape(depth, n, units).transpose(1, 0, 2)
+    gb = gate_weight.reshape(depth, n, units).transpose(1, 0, 2)
+    db = down_weight.reshape(n, units, depth)
+    many = [dma((n,))]
+    att, wu, wg, wd = pl.pallas_call(
+        functools.partial(attention_kernel, n, heads),
+        out_shape=(
+            jax.ShapeDtypeStruct((rows, width), bf),
+            jax.ShapeDtypeStruct((n, depth, units), bf),
+            jax.ShapeDtypeStruct((n, depth, units), bf),
+            jax.ShapeDtypeStruct((units, n * depth), bf),
+        ),
+        in_specs=vm(3) + [pl.BlockSpec(memory_space=pltpu.SMEM)] + vm(4),
+        out_specs=tuple(vm(4)),
+        scratch_shapes=[
+            pltpu.VMEM((heads, rows, VD), bf),
+            pltpu.VMEM((n * rows, VD), bf),
+            pltpu.VMEM((n * rows, VD), bf),
+            pltpu.VMEM((heads, rows, VD), bf),
+            dma((heads,)), dma((heads,)),
+        ]
+        + many * 4
+        + [dma((heads,)), dma((heads,))]
+        + many * 6,
+        compiler_params=params(0),
+        name="attend_rows",
+    )(q, k, v, second_weight, head_gain.reshape(heads, VD), ub, gb, db)
+    return att, wu.reshape(n * depth, units), wg.reshape(n * depth, units), wd
 
 
 def moving_rows(
@@ -377,12 +658,11 @@
     sp_index = lax.axis_index("sp")
     units = up_weight.shape[1] // n
     taps = conv_weight.shape[0]
-    wu = lax.all_to_all(up_weight, "sp", split_axis=1, concat_axis=0, tiled=True)
-    wg = lax.all_to_all(gate_weight, "sp", split_axis=1, concat_axis=0, tiled=True)
-    wd = lax.all_to_all(down_weight, "sp", split_axis=0, concat_axis=1, tiled=True)
     cw = lax.dynamic_slice_in_dim(conv_weight, sp_index * units, units, 1)
     cb = lax.dynamic_slice_in_dim(conv_bias, sp_index * units, units, 0)
-    attended = attend(queries, key_pairs, values, second_weight, head_gain)
+    attended, wu, wg, wd = attend_rows(
+        n, queries, key_pairs, values, second_weight, head_gain, up_weight, gate_weight, down_weight
+    )
     up, gate, mid = gather_rows(n, attended, out_weight, residual, norm_gain, wu, wg)
     count = up.shape[0]
     extended = jnp.pad(up, ((taps - 1, 0), (0, 0)))

time: 585 us -> 298 us (0.51)
  waiting for transfers between devices: 113 us -> 0 us
  Pallas kernels: 356 us -> 280 us
  blocking collectives: 28.6 us -> 0 us
  matrix products: 22.5 us -> 0 us
  other arithmetic: 19 us -> 5.37 us
  between operations: 13.5 us -> 0.04 us
  local copies, waits for them, and re-layouts: 20 us -> 7.88 us
  starting transfers between devices: 12.1 us -> 0 us
    pallas_call x0 -> x1, Pallas kernels: none -> 117 us  [attend_rows(): pl.pallas_call(functools.partial(attention_kernel, n, heads), out_shape=(...]
    pallas_call x1, Pallas kernels: 184 us -> 83.4 us  [gather_rows(): pl.pallas_call(functools.partial(gather_kernel, n), out_shape=(jax.ShapeD...]
    pallas_call x1, Pallas kernels: 172 us -> 79.6 us  [scatter_rows(): pl.pallas_call(functools.partial(scatter_kernel, n), out_shape=jax.ShapeD...]
    all_gather x2 -> x0, waiting for transfers between devices: 65.9 us -> none  [the longest x1 65.9 us: attend(): value_piece = lax.all_gather(values, 'sp', axis=0, tiled=True)]
    all_to_all x2 -> x0, waiting for transfers between devices: 45.5 us -> none  [the longest x1 24.9 us: moving_rows(): lax.all_to_all(down_weight, 'sp', split_axis=0, concat_axis=1, tiled=True)]
    all_to_all x1 -> x0, blocking collectives: 28.6 us -> none  [moving_rows(): lax.all_to_all(gate_weight, 'sp', split_axis=1, concat_axis=0, tiled=True)]
    dot_general x2 -> x0, matrix products: 22.5 us -> none  [the longest x1 11.8 us: compute(): jnp.einsum('qhmd,khmd->hmqk', query, key_rows, preferred_element_type=jnp...]
    reduce_sum x2 -> x0, other arithmetic: 12.4 us -> none  [the longest x1 11.9 us: compute(): totals = jnp.sum(exp_scores, axis=-1)]
  transfers between devices with their start and end apart: 4 -> 0, of which waited for: 3 -> 0; matrix products, arithmetic and copies ran while one was open for 1% -> 0% of each run, Pallas kernels for 0% -> 0%
where the time goes in v2:
time: 298 us; the launch traced here: 294 us
  Pallas kernels  280 us (94%)
  local copies, waits for them, and re-layouts  7.88 us (3%)
  other arithmetic  5.37 us (2%)
    pallas_call x1, Pallas kernels, attend_rows(): pl.pallas_call(functools.partial(attention_kernel, n, heads), out_shape=(...  117 us
    pallas_call x1, Pallas kernels, gather_rows(): pl.pallas_call(functools.partial(gather_kernel, n), out_shape=(jax.ShapeD...  83.4 us
    pallas_call x1, Pallas kernels, scatter_rows(): pl.pallas_call(functools.partial(scatter_kernel, n), out_shape=jax.ShapeD...  79.6 us

profile of v2, /device:TPU:15, one launch (start us, length us, event | category | flops | bytes accessed | tf_op | source)
XLA Modules:
  0.0 293.7 jit_solution(8084387243583243667)
XLA Ops:
  0.0 0.0 copy-start
  0.0 1.5 copy.14
  1.5 1.3 copy.15
  2.8 0.0 copy-done
  2.8 0.3 copy.16
  3.2 1.3 copy.17
  4.5 117.5 %attend_rows.1 = (bf16[192,512]{1,0:T(8,128)(2,1)}, bf16[16,128,176]{2,1,0:T(8,128)(2,1)}, bf16[16,128,176]{2,1,0:T(8,128)(2,1)}, bf16[176,2048]{1,0:T(8,128)(2,1)}) custom-call(bf16[192,512]{1,0:T(8,128)(2,1)} %q.1, bf16[192,512]{1,0:T(8,128)(2,1)} %k.1, bf16[192,512]{1,0:T(8,128)(2,1)} %v.1, f32[4]{0:T(128)} %sw.1, f32[4,128]{1,0:T(4,128)} %bitcast.23, ...), custom_call_target="tpu_custom_call" | custom-call | tf_op jit(solution)/shard_map/attend_rows/pallas_call | solution.py:616
  121.9 83.4 %gather_rows.1 = (bf16[3072,176]{1,0:T(8,128)(2,1)}, bf16[3072,176]{1,0:T(8,128)(2,1)}, bf16[96,2048]{1,0:T(8,128)(2,1)}) custom-call(bf16[192,512]{1,0:T(8,128)(2,1)} %get-tuple-element.12.att, bf16[512,2048]{1,0:T(8,128)(2,1)} %ow.1, bf16[96,2048]{1,0:T(8,128)(2,1)} %res.1, f32[1,2048]{1,0:T(1,128)} %bitcast.19, bf16[2048,176]{1,0:T(8,128)(2,1)} %bitcast.16, ...), custom_call_target="tpu_custom_call" | custom-call | tf_op jit(solution)/shard_map/gather_rows/pallas_call | solution.py:387
  205.3 0.9 constant_dynamic-slice_fusion
  206.2 0.8 dynamic_slice.6
  207.0 5.4 %multiply_convert_fusion.hid = bf16[3072,176]{1,0:T(8,128)(2,1)} fusion(bf16[3072,176]{1,0:T(8,128)(2,1)} %get-tuple-element.16, bf16[3072,176]{1,0:T(8,128)(2,1)} %get-tuple-element.15, f32[176]{0:T(256)S(1)} %bitcast.22, f32[176]{0:T(256)S(1)} %bitcast.21, f32[176]{0:T(256)S(1)} %bitcast.20, f32[176]{0:T(256)S(1)} %dynamic_slice.6), kind=kLoop, calls=%fused_computation | loop fusion | flops 8650752 | bytes 3246848 | tf_op jit(solution)/shard_map/convert_element_type | solution.py:672
  212.3 79.6 %scatter_rows.1 = bf16[96,2048]{1,0:T(8,128)(2,1)} custom-call(bf16[3072,176]{1,0:T(8,128)(2,1)} %multiply_convert_fusion.hid, bf16[176,2048]{1,0:T(8,128)(2,1)} %get-tuple-element.17.down, bf16[96,2048]{1,0:T(8,128)(2,1)} %get-tuple-element.18.mid), custom_call_target="tpu_custom_call" | custom-call | tf_op jit(solution)/shard_map/scatter_rows/pallas_call | solution.py:414
  291.9 1.8 copy.19
Async XLA Ops:
  0.0 2.8 copy-start
